TPU v7x, 128 devices: a whole 4x4x4 slice. The times are simulated.
128 devices in a mesh: sp: 32 (over z, y, core), tp: 4 (over x).
Axes of the slice: x: 4, y: 4, z: 4, core: 2. Of those that a mesh axis runs over, the one named last changes fastest.
Arguments:
- tokens: bfloat16 [16384, 2048], P(('sp', 'tp')), may hold values from -6 to 6
- norm_gain: float32 [2048], replicated, may hold values from 0.25 to 5
- w_query_one: bfloat16 [2048, 512], P(None, 'tp'), may hold values from -0.21875 to 0.21875
- w_query_two: bfloat16 [2048, 512], P(None, 'tp'), may hold values from -0.21875 to 0.21875
- w_key_one: bfloat16 [2048, 512], P(None, 'tp'), may hold values from -0.125 to 0.125
- w_key_two: bfloat16 [2048, 512], P(None, 'tp'), may hold values from -0.125 to 0.125
- w_value: bfloat16 [2048, 1024], P(None, 'tp'), may hold values from -0.125 to 0.125
- mix_lambda: float32 [8], P('tp'), may hold values from 0.3 to 0.8
- head_gain: float32 [128], replicated, may hold values from 0.1 to 1.9
- w_ret_query: bfloat16 [2048, 512], P(None, 'tp'), may hold values from -0.125 to 0.125
- w_ret_key: bfloat16 [2048, 512], P(None, 'tp'), may hold values from -0.125 to 0.125
- w_ret_value: bfloat16 [2048, 1024], P(None, 'tp'), may hold values from -0.125 to 0.125
- retain_log: float32 [8, 16384], P('tp', 'sp'), may hold values from -1 to 0
- init_state: float32 [8, 64, 128], P('tp'), may hold values from -144 to 144
- w_out_diff: bfloat16 [1024, 2048], P('tp'), may hold values from -0.125 to 0.125
- w_out_ret: bfloat16 [1024, 2048], P('tp'), may hold values from -0.125 to 0.125
Outputs:
- mixed: bfloat16 [16384, 2048], P(('sp', 'tp'))
All inputs are finite; a program needn't handle non-finite values.
Results may differ from a plain program's by a relative error of at most 0.015.
The roundings to bfloat16 on the way count: a program that leaves them out, or rounds other values in their place, can miss the bound.
Values may be sent and summed in bfloat16 or wider, within the bound.
A program may use at most 128 MiB of HBM per device.

v0:
```python
import math

import jax
import jax.numpy as jnp
from jax import lax
from jax.sharding import Mesh
from jax.sharding import PartitionSpec as P

BLOCK = 256
SP = ("sp_0", "sp_1", "sp_2")
SP_TP = ("sp_0", "sp_1", "sp_2", "tp")


NORM_EPS = 1e-06
HEAD_EPS = 1e-05
DIFF_SCALE = 0.8


def sent_to_all(x, axis):
    length = lax.axis_size(axis)
    return lax.all_to_all(jnp.broadcast_to(x[None], (length, *x.shape)), axis, 0, 0, tiled=True)


def in_order(tiles, dim):
    dims = list(tiles.shape[1:])
    dims[dim] *= tiles.shape[0]
    return jnp.moveaxis(tiles, 0, dim).reshape(dims)


def gather_directly(x, axis, dim):
    tiles = sent_to_all(x, axis)
    return in_order(tiles, dim)


def filled_with(x, identity):
    return jax.tree.map(
        lambda a, e: jnp.broadcast_to(jnp.asarray(e, a.dtype), a.shape), x, identity
    )


def collected_together(x, axis):
    leaves = jax.tree.leaves(x)
    turns = sorted(range(len(leaves)), key=lambda k: -leaves[k].size)
    width = (1, *leaves[turns[0]].shape)[-1]
    lines = [
        jnp.pad(leaves[k].reshape(-1), (0, -leaves[k].size % width)).reshape(-1, width)
        for k in turns
    ]
    both, at, found = (lax.all_gather(jnp.concatenate(lines), axis), 0, {})
    for k, line in zip(turns, lines):
        slab = both[:, at : at + len(line)].reshape(len(both), -1)
        found[k] = slab[:, : leaves[k].size].reshape(-1, *leaves[k].shape)
        at += len(line)
    numbers = iter(range(len(leaves)))
    return jax.tree.map(lambda _: found[next(numbers)], x)


def entering(x, axes, combine, identity):
    before = start = filled_with(x, identity)
    total = x
    for axis in reversed(axes):
        length, index = (lax.axis_size(axis), lax.axis_index(axis))
        pieces = collected_together(
            jax.tree.map(lambda part, kind: part.astype(kind), total, (jnp.bfloat16, jnp.bfloat16)),
            axis,
        )
        inside, total = (start, start)
        for k in range(length):
            passed = k < index
            total = combine(
                total, jax.tree.map(lambda part, own: part[k].astype(own.dtype), pieces, x)
            )
            inside = jax.tree.map(lambda new, old: jnp.where(passed, new, old), total, inside)
        before = combine(inside, before)
    return before


def side_by_side(arrays, axis, dim, along):
    widths = [a.shape[along] for a in arrays]
    both = jnp.concatenate(arrays, axis=along)
    out = lax.all_gather(both, axis, axis=dim, tiled=True)
    return tuple(jnp.split(out, [sum(widths[:k]) for k in range(1, len(widths))], axis=along))


def head_norm(values):
    return values * lax.rsqrt(jnp.mean(values * values, axis=-1, keepdims=True) + HEAD_EPS)


def soft_update(running, query, keys, values, allowed):
    peak_old, denominator, weighted = running
    scores = jnp.einsum(
        "qhd,khd->hqk", query, keys, preferred_element_type=jnp.float32
    ) * query.shape[-1] ** (-0.5)
    scores = jnp.where(allowed[None], scores, -jnp.inf)
    peak_new = jnp.maximum(peak_old, jnp.max(scores, axis=-1))
    offset = jnp.where(jnp.isinf(peak_new), 0.0, peak_new)
    rescale = jnp.exp(peak_old - offset)
    shifted = jnp.exp(scores - offset[..., None])
    denominator = denominator * rescale + jnp.sum(shifted, axis=-1)
    weighted = weighted * rescale[..., None] + jnp.einsum(
        "hqk,khe->hqe", shifted.astype(jnp.bfloat16), values, preferred_element_type=jnp.float32
    )
    return (peak_new, denominator, weighted)


def on_device(
    tokens,
    norm_gain,
    w_query_one,
    w_query_two,
    w_key_one,
    w_key_two,
    w_value,
    mix_lambda,
    head_gain,
    w_ret_query,
    w_ret_key,
    w_ret_value,
    retain_log,
    init_state,
    w_out_diff,
    w_out_ret,
):
    key_width = w_query_one.shape[1]
    diff_heads = mix_lambda.shape[0]
    head_dim = key_width // diff_heads
    val_dim = head_gain.shape[0]
    value_width = w_value.shape[1]
    ret_heads = init_state.shape[0]
    ret_width = w_ret_query.shape[1]
    floats = tokens.astype(jnp.float32)
    normed = (
        floats * lax.rsqrt(jnp.mean(floats * floats, axis=-1, keepdims=True) + NORM_EPS) * norm_gain
    ).astype(jnp.bfloat16)
    weights = (
        w_query_one,
        w_query_two,
        w_key_one,
        w_key_two,
        w_value,
        w_ret_query,
        w_ret_key,
        w_ret_value,
    )
    portion = gather_directly(normed, "tp", 0)
    projected = jnp.concatenate(
        [
            jnp.dot(portion, weight, preferred_element_type=jnp.float32).astype(jnp.bfloat16)
            for weight in weights
        ],
        axis=1,
    )
    row_count = projected.shape[0]
    query_one = projected[:, :key_width].reshape(row_count, diff_heads, head_dim)
    query_two = projected[:, key_width : 2 * key_width].reshape(row_count, diff_heads, head_dim)
    key_pack = projected[:, 2 * key_width : 4 * key_width + value_width]
    ret_begin = 4 * key_width + value_width
    ret_query = projected[:, ret_begin : ret_begin + ret_width]
    ret_key = projected[:, ret_begin + ret_width : ret_begin + 2 * ret_width]
    ret_value = projected[:, ret_begin + 2 * ret_width :]
    nblocks = row_count // BLOCK

    def split_blocks(data, size):
        return data.reshape(nblocks, BLOCK, ret_heads, size).transpose(0, 2, 1, 3)

    block_query = split_blocks(ret_query, head_dim)
    block_key = split_blocks(ret_key, head_dim)
    block_value = split_blocks(ret_value, val_dim)
    log_blocks = retain_log.reshape(ret_heads, nblocks, BLOCK).transpose(1, 0, 2)
    sequence_index = jnp.arange(BLOCK, dtype=jnp.int32)
    causal = sequence_index[:, None] >= sequence_index[None, :]

    def ret_step(memory, inputs):
        query, keys, values, logs = inputs
        cumulative = jnp.cumsum(logs, axis=-1)
        gap_log = jnp.where(causal[None], cumulative[:, :, None] - cumulative[:, None, :], -jnp.inf)
        raw = jnp.einsum("hqd,hkd->hqk", query, keys, preferred_element_type=jnp.float32)
        decayed = (raw * head_dim ** (-0.5) * jnp.exp(gap_log)).astype(jnp.bfloat16)
        result = jnp.einsum("hqk,hke->hqe", decayed, values, preferred_element_type=jnp.float32)
        result = result + jnp.einsum(
            "hqd,hde->hqe", query.astype(jnp.float32) * jnp.exp(cumulative)[:, :, None], memory
        )
        last_log = cumulative[:, -1:]
        key_scaled = (
            keys.astype(jnp.float32)
            * head_dim ** (-0.5)
            * jnp.exp(last_log - cumulative)[:, :, None]
        ).astype(jnp.bfloat16)
        memory = jnp.exp(last_log)[:, :, None] * memory + jnp.einsum(
            "hkd,hke->hde", key_scaled, values, preferred_element_type=jnp.float32
        )
        return (memory, result)

    zero_state = jnp.zeros((ret_heads, head_dim, val_dim), jnp.float32)
    local_state, local_out = lax.scan(
        ret_step, zero_state, (block_query, block_key, block_value, log_blocks)
    )
    span_log = jnp.sum(retain_log, axis=1)

    def chain_states(first_part, second_part):
        return (
            first_part[0] + second_part[0],
            first_part[1] * jnp.exp(second_part[0])[:, None, None] + second_part[1],
        )

    before_log, before_state = entering(
        (span_log, local_state), SP, chain_states, (jnp.zeros_like(span_log), zero_state)
    )
    carried = before_state + jnp.exp(before_log)[:, None, None] * init_state
    span_cumulative = jnp.cumsum(retain_log, axis=1)
    scaled_query = (
        ret_query.astype(jnp.float32).reshape(row_count, ret_heads, head_dim)
        * jnp.exp(span_cumulative).T[:, :, None]
    )
    ret_heads_out = local_out.transpose(1, 0, 2, 3).reshape(
        ret_heads, row_count, val_dim
    ) + jnp.einsum("thd,hde->hte", scaled_query, carried)
    ret_out = (
        head_norm(ret_heads_out)
        .transpose(1, 0, 2)
        .reshape(row_count, ret_heads * val_dim)
        .astype(jnp.bfloat16)
    )
    place = lax.axis_index(SP)
    query_pos = place * row_count + jnp.arange(row_count, dtype=jnp.int32)
    last_pos = place * row_count + row_count - 1

    def attend(running, key_block, begin_at):
        key_count = key_block.shape[0]
        keys_one = key_block[:, :key_width].reshape(key_count, diff_heads, head_dim)
        keys_two = key_block[:, key_width : 2 * key_width].reshape(key_count, diff_heads, head_dim)
        values = key_block[:, 2 * key_width :].reshape(key_count, diff_heads, val_dim)
        allowed = query_pos[:, None] >= (begin_at + jnp.arange(key_count, dtype=jnp.int32))[None, :]
        return (
            soft_update(running[0], query_one, keys_one, values, allowed),
            soft_update(running[1], query_two, keys_two, values, allowed),
        )

    empty_map = (
        jnp.full((diff_heads, row_count), -jnp.inf, jnp.float32),
        jnp.zeros((diff_heads, row_count), jnp.float32),
        jnp.zeros((diff_heads, row_count, val_dim), jnp.float32),
    )
    portion = lax.all_gather(key_pack, SP, axis=0, tiled=True)
    key_count = portion.shape[0]
    stride = math.gcd(key_count, 512)

    def one_block(number, inner_state):
        first_pos = number * stride
        key_block = lax.dynamic_slice_in_dim(portion, number * stride, stride, 0)
        return lax.cond(
            first_pos <= last_pos,
            lambda kept: attend(kept, key_block, first_pos),
            lambda kept: kept,
            inner_state,
        )

    softmax_maps = lax.fori_loop(0, key_count // stride, one_block, (empty_map, empty_map))
    first_map, second_map = softmax_maps
    mixed_heads = (
        first_map[2] / first_map[1][..., None]
        - mix_lambda[:, None, None] * second_map[2] / second_map[1][..., None]
    )
    diff_out = (
        (head_norm(mixed_heads) * head_gain * DIFF_SCALE)
        .transpose(1, 0, 2)
        .reshape(row_count, diff_heads * val_dim)
        .astype(jnp.bfloat16)
    )
    diff_rows, ret_rows = (
        lax.all_to_all(diff_out, "tp", split_axis=0, concat_axis=1, tiled=True),
        lax.all_to_all(ret_out, "tp", split_axis=0, concat_axis=1, tiled=True),
    )
    whole_diff, whole_ret = side_by_side((w_out_diff, w_out_ret), "tp", 0, 1)
    total = jnp.dot(diff_rows, whole_diff, preferred_element_type=jnp.float32) + jnp.dot(
        ret_rows, whole_ret, preferred_element_type=jnp.float32
    )
    return total.astype(jnp.bfloat16)


def solution(mesh):
    split = Mesh(mesh.devices.reshape(4, 4, 2, mesh.shape["tp"]), ("sp_0", "sp_1", "sp_2", "tp"))
    return jax.shard_map(
        on_device,
        mesh=split,
        in_specs=(
            P(SP_TP, None),
            P(),
            P(None, "tp"),
            P(None, "tp"),
            P(None, "tp"),
            P(None, "tp"),
            P(None, "tp"),
            P("tp"),
            P(),
            P(None, "tp"),
            P(None, "tp"),
            P(None, "tp"),
            P("tp", SP),
            P("tp", None, None),
            P("tp", None),
            P("tp", None),
        ),
        out_specs=P(SP_TP, None),
        check_vma=False,
    )
```

profile of v0, /device:TPU:121, one launch (start us, length us, event | category | flops | bytes accessed | tf_op | source)
XLA Modules:
  0.0 355.8 jit_solution(14863701098823507889)
XLA Ops:
  9.4 29.4 %all_to_all.37 = bf16[4,128,2048]{2,1,0:T(8,128)(2,1)S(1)} all-to-all(bf16[4,128,2048]{2,1,0:T(8,128)(2,1)S(1)} %broadcast_in_dim.67), channel_id=1, replica_groups=mesh['sp_0'=4,'sp_1'=4,'sp_2'=2,'tp'=4] {'tp'}, dimensions={0} | all-to-all | bytes 4194304 | tf_op jit(solution)/shard_map/all_to_all | solution.py:21
  62.8 12.3 %while.38 = (s32[]{:T(128)}, f32[2,64,128]{2,1,0:T(8,128)S(1)}, f32[2,2,256,128]{3,2,1,0:T(8,128)}, f32[2,2,256]{2,1,0:T(2,128)S(1)}, bf16[2,2,256,64]{2,3,1,0:T...) while((s32[]{:T(128)}, f32[2,64,128]{2,1,0:T(8,128)S(1)}, ...), condition=%wide.region_13.14_spmd.clone, body=%wide.region_10.13_spmd.clone.sunk | while | flops 68191240 | bytes 1678610 | solution.py:195
  83.5 10.7 %all-gather.4 = bf16[4,129,128]{2,1,0:T(8,128)(2,1)S(1)} all-gather(bf16[1,129,128]{2,1,0:T(8,128)(2,1)S(1)} %maximum_bitcast_fusion.1), channel_id=3, replica_groups=mesh['sp_0'=4,'sp_1'=4,'sp_2'=2,'tp'=4] {'sp_1'}, dimensions={0}, use_global_device_ids=true | all-gather | bytes 165120 | tf_op jit(solution)/shard_map/all_gather | solution.py:49
  94.9 11.1 %all-gather.5 = bf16[4,129,128]{2,1,0:T(8,128)(2,1)S(1)} all-gather(bf16[1,129,128]{2,1,0:T(8,128)(2,1)S(1)} %maximum_bitcast_fusion.2), channel_id=4, replica_groups=mesh['sp_0'=4,'sp_1'=4,'sp_2'=2,'tp'=4] {'sp_0'}, dimensions={0}, use_global_device_ids=true | all-gather | bytes 165120 | tf_op jit(solution)/shard_map/all_gather | solution.py:49
  122.5 210.9 %while.37 = (s32[]{:T(128)}, f32[2,512]{1,0:T(2,128)S(1)}, f32[2,512]{1,0:T(2,128)S(1)}, f32[2,512,128]{2,1,0:T(8,128)S(1)}, f32[2,512]{1,0:T(2,128)S(1)}, /*ind...) while((s32[]{:T(128)}, f32[2,512]{1,0:T(2,128)S(1)}, ...), condition=%wide.region_8.9_spmd.clone, body=%wide.region_1.8_spmd.clone.sunk | while | flops 410797056 | bytes 17715636 | solution.py:258
  122.5 6.5 %conditional.3 = ((f32[2,512]{1,0:T(2,128)S(1)}, f32[2,512]{1,0:T(2,128)S(1)}, f32[2,512,128]{2,1,0:T(8,128)S(1)}, f32[2,512]{1,0:T(2,128)S(1)}, f32[2,512]{1,0:T(2,128)S(1)}, /*index=5*/f32[2,512,128]{2,1,0:T(8,128)S(1)})) conditional(s32[]{:T(128)} %convert_element_type.554, (f32[2,512]{1,0:T(2,128)S(1)}, f32[2,512]{1,0:T(2,128)S(1)}, ...), branch_computations={%region_2.2_spmd, %region_3.7_spmd} | conditional | flops 410797056 | bytes 17713286 | solution.py:251
  129.1 6.5 %conditional.3 = ((f32[2,512]{1,0:T(2,128)S(1)}, f32[2,512]{1,0:T(2,128)S(1)}, f32[2,512,128]{2,1,0:T(8,128)S(1)}, f32[2,512]{1,0:T(2,128)S(1)}, f32[2,512]{1,0:T(2,128)S(1)}, /*index=5*/f32[2,512,128]{2,1,0:T(8,128)S(1)})) conditional(s32[]{:T(128)} %convert_element_type.554, (f32[2,512]{1,0:T(2,128)S(1)}, f32[2,512]{1,0:T(2,128)S(1)}, ...), branch_computations={%region_2.2_spmd, %region_3.7_spmd} | conditional | flops 410797056 | bytes 17713286 | solution.py:251
  135.7 6.7 %conditional.3 = ((f32[2,512]{1,0:T(2,128)S(1)}, f32[2,512]{1,0:T(2,128)S(1)}, f32[2,512,128]{2,1,0:T(8,128)S(1)}, f32[2,512]{1,0:T(2,128)S(1)}, f32[2,512]{1,0:T(2,128)S(1)}, /*index=5*/f32[2,512,128]{2,1,0:T(8,128)S(1)})) conditional(s32[]{:T(128)} %convert_element_type.554, (f32[2,512]{1,0:T(2,128)S(1)}, f32[2,512]{1,0:T(2,128)S(1)}, ...), branch_computations={%region_2.2_spmd, %region_3.7_spmd} | conditional | flops 410797056 | bytes 17713286 | solution.py:251
  142.4 6.5 %conditional.3 = ((f32[2,512]{1,0:T(2,128)S(1)}, f32[2,512]{1,0:T(2,128)S(1)}, f32[2,512,128]{2,1,0:T(8,128)S(1)}, f32[2,512]{1,0:T(2,128)S(1)}, f32[2,512]{1,0:T(2,128)S(1)}, /*index=5*/f32[2,512,128]{2,1,0:T(8,128)S(1)})) conditional(s32[]{:T(128)} %convert_element_type.554, (f32[2,512]{1,0:T(2,128)S(1)}, f32[2,512]{1,0:T(2,128)S(1)}, ...), branch_computations={%region_2.2_spmd, %region_3.7_spmd} | conditional | flops 410797056 | bytes 17713286 | solution.py:251
  149.0 6.6 %conditional.3 = ((f32[2,512]{1,0:T(2,128)S(1)}, f32[2,512]{1,0:T(2,128)S(1)}, f32[2,512,128]{2,1,0:T(8,128)S(1)}, f32[2,512]{1,0:T(2,128)S(1)}, f32[2,512]{1,0:T(2,128)S(1)}, /*index=5*/f32[2,512,128]{2,1,0:T(8,128)S(1)})) conditional(s32[]{:T(128)} %convert_element_type.554, (f32[2,512]{1,0:T(2,128)S(1)}, f32[2,512]{1,0:T(2,128)S(1)}, ...), branch_computations={%region_2.2_spmd, %region_3.7_spmd} | conditional | flops 410797056 | bytes 17713286 | solution.py:251
  155.6 6.5 %conditional.3 = ((f32[2,512]{1,0:T(2,128)S(1)}, f32[2,512]{1,0:T(2,128)S(1)}, f32[2,512,128]{2,1,0:T(8,128)S(1)}, f32[2,512]{1,0:T(2,128)S(1)}, f32[2,512]{1,0:T(2,128)S(1)}, /*index=5*/f32[2,512,128]{2,1,0:T(8,128)S(1)})) conditional(s32[]{:T(128)} %convert_element_type.554, (f32[2,512]{1,0:T(2,128)S(1)}, f32[2,512]{1,0:T(2,128)S(1)}, ...), branch_computations={%region_2.2_spmd, %region_3.7_spmd} | conditional | flops 410797056 | bytes 17713286 | solution.py:251
  162.2 6.5 %conditional.3 = ((f32[2,512]{1,0:T(2,128)S(1)}, f32[2,512]{1,0:T(2,128)S(1)}, f32[2,512,128]{2,1,0:T(8,128)S(1)}, f32[2,512]{1,0:T(2,128)S(1)}, f32[2,512]{1,0:T(2,128)S(1)}, /*index=5*/f32[2,512,128]{2,1,0:T(8,128)S(1)})) conditional(s32[]{:T(128)} %convert_element_type.554, (f32[2,512]{1,0:T(2,128)S(1)}, f32[2,512]{1,0:T(2,128)S(1)}, ...), branch_computations={%region_2.2_spmd, %region_3.7_spmd} | conditional | flops 410797056 | bytes 17713286 | solution.py:251
  168.8 6.6 %conditional.3 = ((f32[2,512]{1,0:T(2,128)S(1)}, f32[2,512]{1,0:T(2,128)S(1)}, f32[2,512,128]{2,1,0:T(8,128)S(1)}, f32[2,512]{1,0:T(2,128)S(1)}, f32[2,512]{1,0:T(2,128)S(1)}, /*index=5*/f32[2,512,128]{2,1,0:T(8,128)S(1)})) conditional(s32[]{:T(128)} %convert_element_type.554, (f32[2,512]{1,0:T(2,128)S(1)}, f32[2,512]{1,0:T(2,128)S(1)}, ...), branch_computations={%region_2.2_spmd, %region_3.7_spmd} | conditional | flops 410797056 | bytes 17713286 | solution.py:251
  175.4 6.6 %conditional.3 = ((f32[2,512]{1,0:T(2,128)S(1)}, f32[2,512]{1,0:T(2,128)S(1)}, f32[2,512,128]{2,1,0:T(8,128)S(1)}, f32[2,512]{1,0:T(2,128)S(1)}, f32[2,512]{1,0:T(2,128)S(1)}, /*index=5*/f32[2,512,128]{2,1,0:T(8,128)S(1)})) conditional(s32[]{:T(128)} %convert_element_type.554, (f32[2,512]{1,0:T(2,128)S(1)}, f32[2,512]{1,0:T(2,128)S(1)}, ...), branch_computations={%region_2.2_spmd, %region_3.7_spmd} | conditional | flops 410797056 | bytes 17713286 | solution.py:251
  182.0 6.6 %conditional.3 = ((f32[2,512]{1,0:T(2,128)S(1)}, f32[2,512]{1,0:T(2,128)S(1)}, f32[2,512,128]{2,1,0:T(8,128)S(1)}, f32[2,512]{1,0:T(2,128)S(1)}, f32[2,512]{1,0:T(2,128)S(1)}, /*index=5*/f32[2,512,128]{2,1,0:T(8,128)S(1)})) conditional(s32[]{:T(128)} %convert_element_type.554, (f32[2,512]{1,0:T(2,128)S(1)}, f32[2,512]{1,0:T(2,128)S(1)}, ...), branch_computations={%region_2.2_spmd, %region_3.7_spmd} | conditional | flops 410797056 | bytes 17713286 | solution.py:251
  188.6 6.5 %conditional.3 = ((f32[2,512]{1,0:T(2,128)S(1)}, f32[2,512]{1,0:T(2,128)S(1)}, f32[2,512,128]{2,1,0:T(8,128)S(1)}, f32[2,512]{1,0:T(2,128)S(1)}, f32[2,512]{1,0:T(2,128)S(1)}, /*index=5*/f32[2,512,128]{2,1,0:T(8,128)S(1)})) conditional(s32[]{:T(128)} %convert_element_type.554, (f32[2,512]{1,0:T(2,128)S(1)}, f32[2,512]{1,0:T(2,128)S(1)}, ...), branch_computations={%region_2.2_spmd, %region_3.7_spmd} | conditional | flops 410797056 | bytes 17713286 | solution.py:251
  201.7 6.5 %conditional.3 = ((f32[2,512]{1,0:T(2,128)S(1)}, f32[2,512]{1,0:T(2,128)S(1)}, f32[2,512,128]{2,1,0:T(8,128)S(1)}, f32[2,512]{1,0:T(2,128)S(1)}, f32[2,512]{1,0:T(2,128)S(1)}, /*index=5*/f32[2,512,128]{2,1,0:T(8,128)S(1)})) conditional(s32[]{:T(128)} %convert_element_type.554, (f32[2,512]{1,0:T(2,128)S(1)}, f32[2,512]{1,0:T(2,128)S(1)}, ...), branch_computations={%region_2.2_spmd, %region_3.7_spmd} | conditional | flops 410797056 | bytes 17713286 | solution.py:251
  208.3 6.5 %conditional.3 = ((f32[2,512]{1,0:T(2,128)S(1)}, f32[2,512]{1,0:T(2,128)S(1)}, f32[2,512,128]{2,1,0:T(8,128)S(1)}, f32[2,512]{1,0:T(2,128)S(1)}, f32[2,512]{1,0:T(2,128)S(1)}, /*index=5*/f32[2,512,128]{2,1,0:T(8,128)S(1)})) conditional(s32[]{:T(128)} %convert_element_type.554, (f32[2,512]{1,0:T(2,128)S(1)}, f32[2,512]{1,0:T(2,128)S(1)}, ...), branch_computations={%region_2.2_spmd, %region_3.7_spmd} | conditional | flops 410797056 | bytes 17713286 | solution.py:251
  214.9 6.5 %conditional.3 = ((f32[2,512]{1,0:T(2,128)S(1)}, f32[2,512]{1,0:T(2,128)S(1)}, f32[2,512,128]{2,1,0:T(8,128)S(1)}, f32[2,512]{1,0:T(2,128)S(1)}, f32[2,512]{1,0:T(2,128)S(1)}, /*index=5*/f32[2,512,128]{2,1,0:T(8,128)S(1)})) conditional(s32[]{:T(128)} %convert_element_type.554, (f32[2,512]{1,0:T(2,128)S(1)}, f32[2,512]{1,0:T(2,128)S(1)}, ...), branch_computations={%region_2.2_spmd, %region_3.7_spmd} | conditional | flops 410797056 | bytes 17713286 | solution.py:251
  221.5 6.5 %conditional.3 = ((f32[2,512]{1,0:T(2,128)S(1)}, f32[2,512]{1,0:T(2,128)S(1)}, f32[2,512,128]{2,1,0:T(8,128)S(1)}, f32[2,512]{1,0:T(2,128)S(1)}, f32[2,512]{1,0:T(2,128)S(1)}, /*index=5*/f32[2,512,128]{2,1,0:T(8,128)S(1)})) conditional(s32[]{:T(128)} %convert_element_type.554, (f32[2,512]{1,0:T(2,128)S(1)}, f32[2,512]{1,0:T(2,128)S(1)}, ...), branch_computations={%region_2.2_spmd, %region_3.7_spmd} | conditional | flops 410797056 | bytes 17713286 | solution.py:251
  228.1 6.5 %conditional.3 = ((f32[2,512]{1,0:T(2,128)S(1)}, f32[2,512]{1,0:T(2,128)S(1)}, f32[2,512,128]{2,1,0:T(8,128)S(1)}, f32[2,512]{1,0:T(2,128)S(1)}, f32[2,512]{1,0:T(2,128)S(1)}, /*index=5*/f32[2,512,128]{2,1,0:T(8,128)S(1)})) conditional(s32[]{:T(128)} %convert_element_type.554, (f32[2,512]{1,0:T(2,128)S(1)}, f32[2,512]{1,0:T(2,128)S(1)}, ...), branch_computations={%region_2.2_spmd, %region_3.7_spmd} | conditional | flops 410797056 | bytes 17713286 | solution.py:251
  234.6 6.5 %conditional.3 = ((f32[2,512]{1,0:T(2,128)S(1)}, f32[2,512]{1,0:T(2,128)S(1)}, f32[2,512,128]{2,1,0:T(8,128)S(1)}, f32[2,512]{1,0:T(2,128)S(1)}, f32[2,512]{1,0:T(2,128)S(1)}, /*index=5*/f32[2,512,128]{2,1,0:T(8,128)S(1)})) conditional(s32[]{:T(128)} %convert_element_type.554, (f32[2,512]{1,0:T(2,128)S(1)}, f32[2,512]{1,0:T(2,128)S(1)}, ...), branch_computations={%region_2.2_spmd, %region_3.7_spmd} | conditional | flops 410797056 | bytes 17713286 | solution.py:251
  241.2 6.5 %conditional.3 = ((f32[2,512]{1,0:T(2,128)S(1)}, f32[2,512]{1,0:T(2,128)S(1)}, f32[2,512,128]{2,1,0:T(8,128)S(1)}, f32[2,512]{1,0:T(2,128)S(1)}, f32[2,512]{1,0:T(2,128)S(1)}, /*index=5*/f32[2,512,128]{2,1,0:T(8,128)S(1)})) conditional(s32[]{:T(128)} %convert_element_type.554, (f32[2,512]{1,0:T(2,128)S(1)}, f32[2,512]{1,0:T(2,128)S(1)}, ...), branch_computations={%region_2.2_spmd, %region_3.7_spmd} | conditional | flops 410797056 | bytes 17713286 | solution.py:251
  247.8 6.5 %conditional.3 = ((f32[2,512]{1,0:T(2,128)S(1)}, f32[2,512]{1,0:T(2,128)S(1)}, f32[2,512,128]{2,1,0:T(8,128)S(1)}, f32[2,512]{1,0:T(2,128)S(1)}, f32[2,512]{1,0:T(2,128)S(1)}, /*index=5*/f32[2,512,128]{2,1,0:T(8,128)S(1)})) conditional(s32[]{:T(128)} %convert_element_type.554, (f32[2,512]{1,0:T(2,128)S(1)}, f32[2,512]{1,0:T(2,128)S(1)}, ...), branch_computations={%region_2.2_spmd, %region_3.7_spmd} | conditional | flops 410797056 | bytes 17713286 | solution.py:251
  254.4 6.5 %conditional.3 = ((f32[2,512]{1,0:T(2,128)S(1)}, f32[2,512]{1,0:T(2,128)S(1)}, f32[2,512,128]{2,1,0:T(8,128)S(1)}, f32[2,512]{1,0:T(2,128)S(1)}, f32[2,512]{1,0:T(2,128)S(1)}, /*index=5*/f32[2,512,128]{2,1,0:T(8,128)S(1)})) conditional(s32[]{:T(128)} %convert_element_type.554, (f32[2,512]{1,0:T(2,128)S(1)}, f32[2,512]{1,0:T(2,128)S(1)}, ...), branch_computations={%region_2.2_spmd, %region_3.7_spmd} | conditional | flops 410797056 | bytes 17713286 | solution.py:251
  261.0 6.5 %conditional.3 = ((f32[2,512]{1,0:T(2,128)S(1)}, f32[2,512]{1,0:T(2,128)S(1)}, f32[2,512,128]{2,1,0:T(8,128)S(1)}, f32[2,512]{1,0:T(2,128)S(1)}, f32[2,512]{1,0:T(2,128)S(1)}, /*index=5*/f32[2,512,128]{2,1,0:T(8,128)S(1)})) conditional(s32[]{:T(128)} %convert_element_type.554, (f32[2,512]{1,0:T(2,128)S(1)}, f32[2,512]{1,0:T(2,128)S(1)}, ...), branch_computations={%region_2.2_spmd, %region_3.7_spmd} | conditional | flops 410797056 | bytes 17713286 | solution.py:251
  267.6 6.5 %conditional.3 = ((f32[2,512]{1,0:T(2,128)S(1)}, f32[2,512]{1,0:T(2,128)S(1)}, f32[2,512,128]{2,1,0:T(8,128)S(1)}, f32[2,512]{1,0:T(2,128)S(1)}, f32[2,512]{1,0:T(2,128)S(1)}, /*index=5*/f32[2,512,128]{2,1,0:T(8,128)S(1)})) conditional(s32[]{:T(128)} %convert_element_type.554, (f32[2,512]{1,0:T(2,128)S(1)}, f32[2,512]{1,0:T(2,128)S(1)}, ...), branch_computations={%region_2.2_spmd, %region_3.7_spmd} | conditional | flops 410797056 | bytes 17713286 | solution.py:251
  274.2 6.5 %conditional.3 = ((f32[2,512]{1,0:T(2,128)S(1)}, f32[2,512]{1,0:T(2,128)S(1)}, f32[2,512,128]{2,1,0:T(8,128)S(1)}, f32[2,512]{1,0:T(2,128)S(1)}, f32[2,512]{1,0:T(2,128)S(1)}, /*index=5*/f32[2,512,128]{2,1,0:T(8,128)S(1)})) conditional(s32[]{:T(128)} %convert_element_type.554, (f32[2,512]{1,0:T(2,128)S(1)}, f32[2,512]{1,0:T(2,128)S(1)}, ...), branch_computations={%region_2.2_spmd, %region_3.7_spmd} | conditional | flops 410797056 | bytes 17713286 | solution.py:251
  287.3 6.5 %conditional.3 = ((f32[2,512]{1,0:T(2,128)S(1)}, f32[2,512]{1,0:T(2,128)S(1)}, f32[2,512,128]{2,1,0:T(8,128)S(1)}, f32[2,512]{1,0:T(2,128)S(1)}, f32[2,512]{1,0:T(2,128)S(1)}, /*index=5*/f32[2,512,128]{2,1,0:T(8,128)S(1)})) conditional(s32[]{:T(128)} %convert_element_type.554, (f32[2,512]{1,0:T(2,128)S(1)}, f32[2,512]{1,0:T(2,128)S(1)}, ...), branch_computations={%region_2.2_spmd, %region_3.7_spmd} | conditional | flops 410797056 | bytes 17713286 | solution.py:251
  293.9 6.5 %conditional.3 = ((f32[2,512]{1,0:T(2,128)S(1)}, f32[2,512]{1,0:T(2,128)S(1)}, f32[2,512,128]{2,1,0:T(8,128)S(1)}, f32[2,512]{1,0:T(2,128)S(1)}, f32[2,512]{1,0:T(2,128)S(1)}, /*index=5*/f32[2,512,128]{2,1,0:T(8,128)S(1)})) conditional(s32[]{:T(128)} %convert_element_type.554, (f32[2,512]{1,0:T(2,128)S(1)}, f32[2,512]{1,0:T(2,128)S(1)}, ...), branch_computations={%region_2.2_spmd, %region_3.7_spmd} | conditional | flops 410797056 | bytes 17713286 | solution.py:251
  300.5 6.5 %conditional.3 = ((f32[2,512]{1,0:T(2,128)S(1)}, f32[2,512]{1,0:T(2,128)S(1)}, f32[2,512,128]{2,1,0:T(8,128)S(1)}, f32[2,512]{1,0:T(2,128)S(1)}, f32[2,512]{1,0:T(2,128)S(1)}, /*index=5*/f32[2,512,128]{2,1,0:T(8,128)S(1)})) conditional(s32[]{:T(128)} %convert_element_type.554, (f32[2,512]{1,0:T(2,128)S(1)}, f32[2,512]{1,0:T(2,128)S(1)}, ...), branch_computations={%region_2.2_spmd, %region_3.7_spmd} | conditional | flops 410797056 | bytes 17713286 | solution.py:251
  307.1 6.5 %conditional.3 = ((f32[2,512]{1,0:T(2,128)S(1)}, f32[2,512]{1,0:T(2,128)S(1)}, f32[2,512,128]{2,1,0:T(8,128)S(1)}, f32[2,512]{1,0:T(2,128)S(1)}, f32[2,512]{1,0:T(2,128)S(1)}, /*index=5*/f32[2,512,128]{2,1,0:T(8,128)S(1)})) conditional(s32[]{:T(128)} %convert_element_type.554, (f32[2,512]{1,0:T(2,128)S(1)}, f32[2,512]{1,0:T(2,128)S(1)}, ...), branch_computations={%region_2.2_spmd, %region_3.7_spmd} | conditional | flops 410797056 | bytes 17713286 | solution.py:251
  (697 shorter events, 318.7 us)
Async XLA Ops:
  6.5 34.1 %copy-start = (bf16[2048,256]{1,0:T(8,128)(2,1)S(1)}, bf16[2048,256]{1,0:T(8,128)(2,1)}, u32[]{:S(2)}) copy-start(bf16[2048,256]{1,0:T(8,128)(2,1)} %param.28) | copy-start | bytes 3145732
  6.5 115.8 %all-gather.9.cloned.1.call-start = ((), (), s32[]{:S(2)}) async-start(), calls=%async_computation.3 | async-start | bytes 17301504 | tf_op jit(solution)/shard_map/all_gather | solution.py:244
  9.4 29.4 %copy-start.3 = (bf16[2048,128]{1,0:T(8,128)(2,1)S(1)}, bf16[2048,128]{1,0:T(8,128)(2,1)}, u32[]{:S(2)}) copy-start(bf16[2048,128]{1,0:T(8,128)(2,1)} %param.27) | copy-start | bytes 1572868
  38.8 1.0 copy-start.4
  42.3 297.2 %all-gather.11.cloned.1.call-start = ((), (), s32[]{:S(2)}) async-start(), calls=%async_computation.4 | async-start | bytes 10485760 | tf_op jit(solution)/shard_map/all_gather | solution.py:81
  45.5 0.7 copy-start.6
  50.4 9.1 %copy-start.1 = (bf16[512,128]{0,1:T(8,128)(2,1)}, bf16[512,128]{0,1:T(8,128)(2,1)S(1)}, u32[]{:S(2)}) copy-start(bf16[512,128]{0,1:T(8,128)(2,1)S(1)} %convolution_convert_fusion.2) | copy-start | bytes 393220
  75.2 4.4 %copy-start.9 = (bf16[1,128]{1,0:T(2,128)(2,1)S(1)}, bf16[1,128]{1,0:T(2,128)(2,1)}, u32[]{:S(2)}) copy-start(bf16[1,128]{1,0:T(2,128)(2,1)} %pad_bitcast_fusion.2) | copy-start | bytes 772
  75.2 31.0 %copy-start.2 = (bf16[512,128]{0,1:T(8,128)(2,1)S(1)}, bf16[512,128]{0,1:T(8,128)(2,1)}, u32[]{:S(2)}) copy-start(bf16[512,128]{0,1:T(8,128)(2,1)} %copy-done.1) | copy-start | bytes 393220
  75.2 31.0 %copy-start.7 = (f32[1,2,4,128]{3,1,2,0:T(2,128)S(1)}, f32[1,2,4,128]{3,1,2,0:T(2,128)}, u32[]{:S(2)}) copy-start(f32[1,2,4,128]{3,1,2,0:T(2,128)} %copy.76) | copy-start | bytes 12292
  110.3 225.0 %all-to-all-start.2 = ((bf16[4,128,256]{1,2,0:T(8,128)(2,1)}), bf16[4,128,256]{1,2,0:T(8,128)(2,1)S(1)}, u32[]{:S(2)}, u32[]{:S(2)}) async-start(bf16[4,128,256]{1,2,0:T(8,128)(2,1)} %copy.51), calls=%async_computation.2 | async-start | bytes 524288 | tf_op jit(solution)/shard_map/all_to_all | solution.py:272
  113.9 1.9 copy-start.5
  122.5 211.0 %copy-start.8 = (f32[2]{0:T(128)S(1)}, f32[2]{0:T(128)}, u32[]{:S(2)}) copy-start(f32[2]{0:T(128)} %param.29) | copy-start | bytes 28
  122.5 211.5 %copy-start.10 = (f32[128]{0:T(128)S(1)}, f32[128]{0:T(128)}, u32[]{:S(2)}) copy-start(f32[128]{0:T(128)} %param.30) | copy-start | bytes 1540
  335.3 9.7 %all-to-all-start.1 = ((bf16[4,128,256]{2,1,0:T(8,128)(2,1)}), bf16[4,128,256]{2,1,0:T(8,128)(2,1)S(1)}, u32[]{:S(2)}, u32[]{:S(2)}) async-start(bf16[4,128,256]{2,1,0:T(8,128)(2,1)} %convert_element_type.349), calls=%async_computation.1 | async-start | bytes 524288 | tf_op jit(solution)/shard_map/all_to_all | solution.py:271
Sparse Core Ops, SparseCore 0:
  42.5 79.8 all-gather.8
  124.0 84.5 all-gather.10
where the time goes:
time: 359 us; the launch traced here: 356 us
  matrix products  144 us (40%)
  local copies, waits for them, and re-layouts  84.3 us (23%)
  blocking collectives  54.6 us (15%)
  other arithmetic  38.9 us (11%)
  between operations  13.8 us (4%)
  starting transfers between devices  7.82 us (2%)
  waiting for transfers between devices  7.6 us (2%)
  loops' own time  4.8 us (1%)
    dot_general x64, matrix products, soft_update(): jnp.einsum('qhd,khd->hqk', query, keys, preferred_element_type=jnp.float32)  68.7 us
    dot_general x64, matrix products, soft_update(): jnp.einsum('hqk,khe->hqe', shifted.astype(jnp.bfloat16), values, preferre...  45.7 us
    slice x32, local copies, waits for them, and re-layouts, attend(): key_block[:, key_width:2 * key_width]  31.9 us
    slice x32, local copies, waits for them, and re-layouts, attend(): key_block[:, 2 * key_width:].reshape(key_count, diff_heads, val_dim)  31.3 us
    all_to_all x1, blocking collectives, sent_to_all(): lax.all_to_all(jnp.broadcast_to(x[None], (length, *x.shape)), axis, 0, 0,...  29.4 us
    all_gather x3, blocking collectives, collected_together(): both, at, found = (lax.all_gather(jnp.concatenate(lines), axis), 0, {})  25.2 us
    reduce_sum x64, other arithmetic, soft_update(): denominator = denominator * rescale + jnp.sum(shifted, axis=-1)  19.4 us
    dot_general x8, matrix products, on_device(): jnp.dot(portion, weight, preferred_element_type=jnp.float32)  12.8 us
  transfers between devices with their start and end apart: 4, of which 2 were waited for; matrix products, arithmetic and copies ran while one was open for 72% of the time, Pallas kernels for 0%

commit v1 on v0

v1 whole, which is shorter than its diff:
```python
import jax
import jax.numpy as jnp
from jax import lax
from jax.experimental import pallas as pl
from jax.experimental.pallas import tpu as pltpu
from jax.sharding import PartitionSpec as P

NORM_EPS = 1e-06
HEAD_EPS = 1e-05
DIFF_SCALE = 0.8
MESH = pl.DeviceIdType.MESH
F32 = jnp.float32
BF16 = jnp.bfloat16
HIGHEST = lax.Precision.HIGHEST
LOWEST = -3.0e38

ORDER = (
    (0, 0), (0, 1), (0, -1), (1, 0), (-1, 0), (0, 2), (2, 0), (1, 1),
    (1, -1), (-1, 1), (-1, -1), (1, 2), (2, 1), (-1, 2), (2, -1), (2, 2),
)
PLUS_Y, MINUS_Y, PLUS_Z, MINUS_Z = range(4)


def nt(a, b, precision=None):
    return lax.dot_general(
        a, b, (((1,), (1,)), ((), ())), preferred_element_type=F32, precision=precision
    )


def mm(a, b, precision=None):
    return jnp.dot(a, b, preferred_element_type=F32, precision=precision)


def head_norm(values, axis):
    return values * lax.rsqrt(jnp.mean(values * values, axis=axis, keepdims=True) + HEAD_EPS)


def kernel(
    tokens, gain, wq1, wq2, wk1, wk2, wv, mix, hgain, wrq, wrk, wrv, logs, init, wod, wor,
    out,
    rows, weights, proj, kva, kvb, wout, lgs, qrecv, qpad, acc, peak, denom, local, rgate,
    dsend, rsend, heads,
    load_sem, x_send, x_recv, w_send, w_recv, l_send, l_recv, lsib_send, kv_send, kv_recv,
    sib_send, q_sem, o_send, o_recv,
):
    sp = lax.axis_index("sp")
    t = lax.axis_index("tp")
    z, y, c = lax.div(sp, 8), lax.rem(lax.div(sp, 2), 4), lax.rem(sp, 2)
    partner = 31 - sp
    sib = (sp + 1 - 2 * c, t)
    kv = (kva, kvb)

    def place(dz, dy, lane):
        return (lax.rem(z + dz + 4, 4) * 4 + lax.rem(y + dy + 4, 4)) * 2 + lane

    near = (
        (place(0, 1, c), t), (place(0, -1, c), t), (place(1, 0, c), t), (place(-1, 0, c), t),
    )
    xs = [(sp, lax.rem(t + d, 4)) for d in range(4)]

    loads = []
    sources = (
        (wq1, 0, 128), (wq2, 128, 128), (wk1, 256, 128), (wk2, 384, 128), (wv, 512, 256),
        (wrq, 768, 128), (wrk, 896, 128), (wrv, 1024, 256),
    )
    for k, (ref, at, width) in enumerate(sources):
        loads.append(pltpu.make_async_copy(ref, weights.at[:, pl.ds(at, width)], load_sem.at[k]))
    for k, ref in enumerate((wod, wor)):
        loads.append(pltpu.make_async_copy(ref, wout.at[t, k], load_sem.at[8 + k]))
    for load in loads:
        load.start()

    barrier = pltpu.get_barrier_semaphore()
    peers = [xs[1], xs[2], xs[3], sib, *near] + [(partner, d) for d in range(4)]
    for peer in peers:
        pl.semaphore_signal(barrier, inc=1, device_id=peer, device_id_type=MESH)

    for chunk in range(2):
        floats = tokens[chunk * 64 : chunk * 64 + 64].astype(F32)
        scale = lax.rsqrt(jnp.mean(floats * floats, axis=-1, keepdims=True) + NORM_EPS)
        rows[t, chunk * 64 : chunk * 64 + 64] = (floats * scale * gain[...]).astype(BF16)
    lg = logs[...]
    total = jnp.sum(lg, axis=1, keepdims=True)
    head_row = lax.broadcasted_iota(jnp.int32, (8, 128), 0)
    lgs[sp] = jnp.where(head_row == 0, total[0:1], total[1:2])

    pl.semaphore_wait(barrier, len(peers))

    def remote(src, dst, ssem, rsem, dev):
        return pltpu.make_async_remote_copy(
            src_ref=src, dst_ref=dst, send_sem=ssem, recv_sem=rsem, device_id=dev,
            device_id_type=MESH,
        )

    def x_copy(slot, chunk, way, n):
        piece = rows.at[slot, pl.ds(chunk * 64, 64)]
        return remote(piece, piece, x_send.at[n], x_recv.at[slot, chunk], xs[way])

    def w_copy(slot, parts, way, n):
        piece = wout.at[slot, c] if parts is None else wout.at[slot, c, pl.ds(parts * 128, 128)]
        rsem = w_recv.at[slot, 0 if parts is None else parts]
        return remote(piece, piece, w_send.at[n], rsem, xs[way])

    def w_sib(slot, n, kind):
        piece = wout.at[slot, kind]
        return remote(piece, piece, w_send.at[4 + n], w_recv.at[slot, 2], sib)

    l_sends = []

    def l_copy(dz, dy, way):
        j = place(dz, dy, c)
        n = len(l_sends)
        copy = remote(lgs.at[j], lgs.at[j], l_send.at[n], l_recv.at[j], near[way])
        l_sends.append(n)
        copy.start()

    l_sibs = []

    def l_sib(dz, dy):
        j = place(dz, dy, c)
        n = len(l_sibs)
        l_sibs.append(n)
        remote(lgs.at[j], lgs.at[j], lsib_send.at[n], l_recv.at[j], sib).start()

    def l_wait(dz, dy, lane=None):
        j = place(dz, dy, c if lane is None else lane)
        remote(lgs.at[j], lgs.at[j], l_send.at[0], l_recv.at[j], sib).wait_recv()

    def l_stage(stage):
        if stage == 0:
            for way in range(4):
                l_copy(0, 0, way)
            l_sib(0, 0)
        elif stage == 1:
            for dy in (1, -1):
                l_wait(0, dy)
                l_copy(0, dy, PLUS_Z)
                l_copy(0, dy, MINUS_Z)
                l_sib(0, dy)
            l_copy(0, -1, PLUS_Y)
            for dz in (1, -1):
                l_wait(dz, 0)
                l_sib(dz, 0)
            l_copy(-1, 0, PLUS_Z)
        elif stage == 2:
            l_wait(0, 2)
            l_copy(0, 2, PLUS_Z)
            l_copy(0, 2, MINUS_Z)
            l_sib(0, 2)
            for dy in (1, -1):
                for dz in (1, -1):
                    l_wait(dz, dy)
                    l_sib(dz, dy)
                l_copy(-1, dy, PLUS_Z)
            l_wait(2, 0)
            l_sib(2, 0)
        elif stage == 3:
            for dz in (1, -1):
                l_wait(dz, 2)
                l_sib(dz, 2)
            l_copy(-1, 2, PLUS_Z)
            for dy in (1, -1):
                l_wait(2, dy)
                l_sib(2, dy)
        else:
            l_wait(2, 2)
            l_sib(2, 2)

    x_copy(t, 0, 1, 0).start()
    x_copy(t, 1, 3, 1).start()
    x_copy(t, 1, 1, 2).start()
    x_copy(t, 0, 3, 3).start()
    l_stage(0)

    for load in loads[:8]:
        load.wait()

    left, right, far = lax.rem(t + 3, 4), lax.rem(t + 1, 4), lax.rem(t + 2, 4)

    def project(k, carry):
        @pl.when(k == 1)
        def _():
            x_copy(left, 0, 1, 0).wait_recv()
            x_copy(left, 0, 1, 4).start()
            x_copy(right, 1, 3, 0).wait_recv()
            x_copy(right, 1, 3, 5).start()
            x_copy(left, 1, 1, 0).wait_recv()
            l_stage(1)

        @pl.when(k == 2)
        def _():
            x_copy(right, 0, 3, 0).wait_recv()
            l_stage(2)
            for load in loads[8:]:
                load.wait()
            w_copy(t, None, 1, 0).start()
            w_copy(t, None, 3, 1).start()

        @pl.when(k == 3)
        def _():
            l_stage(3)
            x_copy(far, 0, 1, 0).wait_recv()
            x_copy(far, 1, 3, 0).wait_recv()

        slot = lax.rem(t + jnp.where(k == 1, 3, jnp.where(k == 2, 1, jnp.where(k == 3, 2, 0))), 4)
        at = pl.multiple_of(slot * 128, 128)
        for n in range(5):
            block = mm(rows[slot], weights[:, n * 256 : n * 256 + 256])
            proj[n, pl.ds(at, 128)] = block.astype(BF16)
        return carry

    lax.fori_loop(0, 4, project, 0)
    l_stage(4)

    def transposed(n, e):
        return proj[n, e * 256 : e * 256 + 256].astype(F32).T.astype(BF16)

    kva[sp, 0] = proj[1, 0:256]
    kva[sp, 1] = transposed(2, 0)
    for way in (PLUS_Y, MINUS_Y, PLUS_Z, MINUS_Z):
        remote(
            kva.at[sp], kva.at[sp], kv_send.at[way, 0], kv_recv.at[sp, 0, 0], near[way]
        ).start()

    local[1] = transposed(0, 1)
    q_copy = remote(local.at[1], qrecv, q_sem.at[0], q_sem.at[1], (partner, t))
    q_copy.start()

    row = lax.broadcasted_iota(jnp.int32, (256, 256), 0)
    col = lax.broadcasted_iota(jnp.int32, (256, 256), 1)
    lane = lax.broadcasted_iota(jnp.int32, (256, 128), 1)
    state_row = lax.broadcasted_iota(jnp.int32, (128, 128), 0)
    upper = jnp.where(row <= col, 1.0, 0.0)
    adds, fades, queries = [], [], []
    for b in range(2):
        span = slice(b * 256, b * 256 + 256)
        lb = lg[:, span]
        cum_rows = mm(jnp.concatenate([lb, lb, lb, lb], axis=0), upper, HIGHEST)
        rq, rk = proj[3, span, 0:128], proj[3, span, 128:256]
        cols, lasts = [], []
        for h in range(2):
            cum_col = jnp.sum(jnp.where(col <= row, lb[h : h + 1], 0.0), axis=1, keepdims=True)
            cols.append(cum_col)
            lasts.append(jnp.sum(lb[h : h + 1], axis=1, keepdims=True))
            mine = (lane < 64) if h == 0 else (lane >= 64)
            raw = nt(jnp.where(mine, rq, jnp.zeros_like(rq)), rk)
            gap = jnp.where(col <= row, cum_col - cum_rows[h : h + 1], -jnp.inf)
            gate = (raw * 0.125 * jnp.exp(gap)).astype(BF16)
            rgate[b, h] = mm(gate, proj[4, span, h * 128 : h * 128 + 128])
        factor = jnp.where(lane < 64, jnp.exp(lasts[0] - cols[0]), jnp.exp(lasts[1] - cols[1]))
        keys = (rk.astype(F32) * 0.125 * factor).T.astype(BF16)
        both = mm(keys, proj[4, span])
        adds.append(jnp.where(state_row < 64, both[:, 0:128], both[:, 128:256]))
        fades.append(jnp.where(state_row < 64, jnp.exp(lasts[0]), jnp.exp(lasts[1])))
        grow = jnp.where(lane < 64, jnp.exp(cols[0]), jnp.exp(cols[1]))
        queries.append(rq.astype(F32) * grow)
    own_state = (fades[1] * adds[0] + adds[1]).astype(BF16)
    pack = jnp.concatenate([own_state[0:64], own_state[64:128]], axis=1)

    kvb[sp, 0, 0:256] = proj[1, 256:512]
    kvb[sp, 1, 0:256] = transposed(2, 1)
    kvb[sp, 0, 256:288] = pack[0:32]
    kvb[sp, 1, 256:288] = pack[32:64]
    for way in (PLUS_Z, MINUS_Z, PLUS_Y, MINUS_Y):
        remote(
            kvb.at[sp], kvb.at[sp], kv_send.at[way, 1], kv_recv.at[sp, 1, 0], near[way]
        ).start()

    sib_number = {}

    def to_sib(e, dz, dy):
        j = place(dz, dy, c)
        n = sib_number.setdefault((e, dz, dy), len(sib_number))
        remote(kv[e].at[j], kv[e].at[j], sib_send.at[n], kv_recv.at[j, e, 0], sib).start()

    ways_used = [2, 2, 2, 2]
    sends = []

    def whole(e, dz, dy, way):
        j = place(dz, dy, c)
        n = ways_used[way]
        ways_used[way] += 1
        sends.append((way, n, e, None))
        remote(kv[e].at[j], kv[e].at[j], kv_send.at[way, n], kv_recv.at[j, e, 0], near[way]).start()

    def part(e, dz, dy, p, way):
        j = place(dz, dy, c)
        n = ways_used[way]
        ways_used[way] += 1
        sends.append((way, n, e, p))
        remote(
            kv[e].at[j, p], kv[e].at[j, p], kv_send.at[way, n], kv_recv.at[j, e, p], near[way]
        ).start()

    def wait_whole(e, dz, dy, from_lane=None):
        j = place(dz, dy, c if from_lane is None else from_lane)
        remote(kv[e].at[j], kv[e].at[j], kv_send.at[0, 0], kv_recv.at[j, e, 0], sib).wait_recv()

    def wait_parts(e, dz, dy):
        j = place(dz, dy, c)
        for p in range(2):
            remote(
                kv[e].at[j, p], kv[e].at[j, p], kv_send.at[0, 0], kv_recv.at[j, e, p], sib
            ).wait_recv()

    to_sib(0, 0, 0)
    to_sib(1, 0, 0)

    def queries_of(half, block):
        big = block.astype(F32) * 0.125
        for hm in range(4):
            own = lax.div(row, 64) == hm
            qpad[half, hm] = jnp.where(own, big, 0.0).astype(BF16)

    queries_of(0, transposed(0, 0))
    for half in range(2):
        for hm in range(4):
            peak[half, hm] = jnp.full((1, 256), LOWEST, F32)
            denom[half, hm] = jnp.zeros((1, 256), F32)
            acc[half, hm] = jnp.zeros((128, 256), F32)
    q_copy.wait_recv()
    queries_of(1, qrecv[...])

    def attend(half, j, masked):
        def scores(hm):
            return [mm(kv[e][j, 0, 0:256], qpad[half, hm]) for e in range(2)]

        later = scores(0)
        for hm in range(4):
            now = later
            if hm < 3:
                later = scores(hm + 1)
            if masked:
                now = [
                    jnp.where(row + e * 256 <= col + half * 256, now[e], -jnp.inf) for e in range(2)
                ]
            old = peak[half, hm]
            new = jnp.maximum(old, jnp.max(jnp.maximum(now[0], now[1]), axis=0, keepdims=True))
            fade = jnp.exp(old - new)
            terms = [jnp.exp(now[e] - new) for e in range(2)]
            denom[half, hm] = denom[half, hm] * fade + jnp.sum(
                terms[0] + terms[1], axis=0, keepdims=True
            )
            h = hm % 2
            weighted = sum(
                mm(kv[e][j, 1, h * 128 : h * 128 + 128], terms[e].astype(BF16)) for e in range(2)
            )
            acc[half, hm] = acc[half, hm] * fade + weighted
            peak[half, hm] = new

    def event(n):
        if n == 2:
            for dy in (1, -1):
                wait_whole(0, 0, dy)
            part(0, 0, -1, 0, PLUS_Y)
            part(0, 0, 1, 1, MINUS_Y)
            for dz in (1, -1):
                wait_whole(0, dz, 0)
            part(0, -1, 0, 0, PLUS_Z)
            part(0, 1, 0, 1, MINUS_Z)
            for d in (1, -1):
                to_sib(0, 0, d)
                to_sib(0, d, 0)
        elif n == 4:
            for dz in (1, -1):
                wait_whole(1, dz, 0)
            part(1, -1, 0, 0, PLUS_Z)
            part(1, 1, 0, 1, MINUS_Z)
            for dy in (1, -1):
                wait_whole(1, 0, dy)
            part(1, 0, -1, 0, PLUS_Y)
            part(1, 0, 1, 1, MINUS_Y)
            for d in (1, -1):
                for way in (PLUS_Z, MINUS_Z):
                    whole(0, 0, d, way)
                for way in (PLUS_Y, MINUS_Y):
                    whole(1, d, 0, way)
            for d in (1, -1):
                to_sib(1, 0, d)
                to_sib(1, d, 0)
        elif n == 6:
            wait_parts(0, 0, 2)
            for way in (PLUS_Z, MINUS_Z):
                whole(0, 0, 2, way)
            wait_parts(1, 2, 0)
            for way in (PLUS_Y, MINUS_Y):
                whole(1, 2, 0, way)
            wait_parts(0, 2, 0)
            wait_parts(1, 0, 2)
            for e in range(2):
                to_sib(e, 0, 2)
                to_sib(e, 2, 0)
        elif n in (8, 10, 12):
            d = {8: 1, 10: -1, 12: 2}[n]
            for s in (1, -1):
                wait_whole(0, s, d)
                wait_whole(1, d, s)
            part(0, -1, d, 0, PLUS_Z)
            part(0, 1, d, 1, MINUS_Z)
            part(1, d, -1, 0, PLUS_Y)
            part(1, d, 1, 1, MINUS_Y)
            for s in (1, -1):
                to_sib(0, s, d)
                to_sib(1, d, s)
        else:
            d = {13: 1, 14: -1, 15: 2}[n]
            wait_parts(0, 2, d)
            wait_parts(1, d, 2)
            to_sib(0, 2, d)
            to_sib(1, d, 2)

    def w_stage(stage):
        if stage == 1:
            w_copy(left, None, 1, 0).wait_recv()
            w_copy(left, 0, 1, 2).start()
            w_copy(right, None, 3, 0).wait_recv()
            w_copy(right, 1, 3, 3).start()
            w_sib(left, 0, c).start()
            w_sib(right, 1, c).start()
        else:
            w_copy(far, 0, 1, 0).wait_recv()
            w_copy(far, 1, 3, 0).wait_recv()
            w_sib(far, 2, c).start()

    bounds = (sp, partner)

    def pick(values, s):
        chosen = jnp.int32(values[0])
        for k, value in enumerate(values[1:], 1):
            chosen = jnp.where(s == k, jnp.int32(value), chosen)
        return chosen

    def step(s, carry):
        for at, events in ((1, (2, 4)), (5, (6,)), (7, (8,)), (8, (10,)), (11, (12, 13)), (13, (14,)), (15, (15,))):
            @pl.when(s == at)
            def _():
                for n in events:
                    event(n)
                if at == 8:
                    w_stage(1)
                if at == 13:
                    w_stage(2)

        dz, dy = pick([o[0] for o in ORDER], s), pick([o[1] for o in ORDER], s)

        def one_lane(l, carry):
            lane_of = lax.rem(c + l, 2)
            j = place(dz, dy, lane_of)

            @pl.when(l == 1)
            def _():
                for e in range(2):
                    remote(
                        kv[e].at[j], kv[e].at[j], kv_send.at[0, 0], kv_recv.at[j, e, 0], sib
                    ).wait_recv()

            def one_half(half, carry):
                bound = jnp.where(half == 0, bounds[0], bounds[1])

                @pl.when(j < bound)
                def _():
                    attend(half, j, False)

                @pl.when(j == bound)
                def _():
                    attend(half, j, True)

                return carry

            return lax.fori_loop(0, 2, one_half, carry)

        return lax.fori_loop(0, 2, one_lane, carry)

    lax.fori_loop(0, 16, step, 0)
    assert ways_used == [10] * 4 and len(sends) == 32 and len(sib_number) == 32
    assert len(l_sends) == 15 and len(l_sibs) == 16

    def finish(half):
        sides = []
        for h in range(2):
            weight_two = mix[pl.ds(h, 1), :]
            first = acc[half, h] / denom[half, h]
            second = acc[half, 2 + h] / denom[half, 2 + h]
            attn = first - weight_two * second
            normal = (head_norm(attn, 0) * DIFF_SCALE).T * hgain[...]
            sides.append(normal)
        dsend[half] = jnp.concatenate(sides, axis=1).astype(BF16)

    def o_copy(kind, src, dev, n):
        return remote(src, heads.at[kind, t], o_send.at[n], o_recv.at[kind, t], dev)

    def o_local(kind, src, n):
        return pltpu.make_async_copy(src, heads.at[kind, t], o_send.at[n])

    finish(0)
    for d in range(2):
        piece = dsend.at[0, pl.ds(d * 128, 128)]

        @pl.when(t == d)
        def _():
            o_local(0, piece, d).start()

        @pl.when(t != d)
        def _():
            o_copy(0, piece, (sp, d), d).start()

    finish(1)
    for d in range(2):
        o_copy(0, dsend.at[1, pl.ds(d * 128, 128)], (partner, 2 + d), 2 + d).start()

    def chain(j, state):
        fade = jnp.exp(lgs[j])
        pair = jnp.concatenate([kvb[j, 0, 256:288], kvb[j, 1, 256:288]], axis=0).astype(F32)
        own = jnp.concatenate([pair[:, 0:128], pair[:, 128:256]], axis=0)
        return state * jnp.where(state_row < 64, fade[0:1], fade[1:2]) + own

    for dz, dy in ORDER:
        l_wait(dz, dy, 1 - c)
    state = lax.fori_loop(0, sp, chain, jnp.concatenate([init[0], init[1]], axis=0))
    for b in range(2):
        for h in range(2):
            mine = (lane < 64) if h == 0 else (lane >= 64)
            older = mm(jnp.where(mine, queries[b], 0.0), state, HIGHEST)
            r = rgate[b, h] + older
            rsend[b * 256 : b * 256 + 256, h * 128 : h * 128 + 128] = head_norm(r, 1).astype(BF16)
        state = fades[b] * state + adds[b]
    for d in range(4):
        piece = rsend.at[pl.ds(d * 128, 128)]

        @pl.when(t == d)
        def _():
            o_local(1, piece, 4 + d).start()

        @pl.when(t != d)
        def _():
            o_copy(1, piece, (sp, d), 4 + d).start()

    for slot, _ in ((left, 0), (right, 1), (far, 2)):
        piece = wout.at[slot, 1 - c]
        remote(piece, piece, w_send.at[0], w_recv.at[slot, 2], sib).wait_recv()

    for slot in range(4):
        landed = remote(heads.at[0, slot], heads.at[0, slot], o_send.at[0], o_recv.at[0, slot], sib)

        @pl.when(jnp.logical_or(t != slot, t >= 2))
        def _():
            landed.wait_recv()

        ret = remote(heads.at[1, slot], heads.at[1, slot], o_send.at[0], o_recv.at[1, slot], sib)

        @pl.when(t != slot)
        def _():
            ret.wait_recv()

    for n in range(2):
        piece = dsend.at[0, pl.ds(n * 128, 128)]

        @pl.when(t == n)
        def _():
            o_local(0, piece, n).wait()

        @pl.when(t != n)
        def _():
            o_copy(0, piece, sib, n).wait_send()

        o_copy(0, piece, sib, 2 + n).wait_send()
    for n in range(4):
        piece = rsend.at[pl.ds(n * 128, 128)]

        @pl.when(t == n)
        def _():
            o_local(1, piece, 4 + n).wait()

        @pl.when(t != n)
        def _():
            o_copy(1, piece, sib, 4 + n).wait_send()

    def columns(n, carry):
        at = pl.ds(pl.multiple_of(n * 512, 512), 512)
        block = jnp.zeros((128, 512), F32)
        for slot in range(4):
            for kind in range(2):
                block += mm(heads[kind, slot], wout[slot, kind, :, at])
        out[:, at] = block.astype(BF16)
        return carry

    lax.fori_loop(0, 4, columns, 0)

    for n in range(6):
        x_copy(t, 0, 1, n).wait_send()
    for n in range(2):
        w_copy(t, None, 1, n).wait_send()
        w_copy(t, n, 1, 2 + n).wait_send()
    for n in range(3):
        w_sib(t, n, c).wait_send()
    for n in l_sends:
        remote(lgs.at[0], lgs.at[0], l_send.at[n], l_recv.at[0], sib).wait_send()
    for n in l_sibs:
        remote(lgs.at[0], lgs.at[0], lsib_send.at[n], l_recv.at[0], sib).wait_send()
    q_copy.wait_send()
    for way in range(4):
        for e in range(2):
            remote(
                kv[e].at[0], kv[e].at[0], kv_send.at[way, e], kv_recv.at[0, 0, 0], sib
            ).wait_send()
    for way, n, e, p in sends:
        piece = kv[e].at[0] if p is None else kv[e].at[0, 0]
        remote(piece, piece, kv_send.at[way, n], kv_recv.at[0, 0, 0], sib).wait_send()
    for (e, _, _), n in sib_number.items():
        remote(kv[e].at[0], kv[e].at[0], sib_send.at[n], kv_recv.at[0, 0, 0], sib).wait_send()


def on_device(
    tokens, norm_gain, w_query_one, w_query_two, w_key_one, w_key_two, w_value, mix_lambda,
    head_gain, w_ret_query, w_ret_key, w_ret_value, retain_log, init_state, w_out_diff, w_out_ret,
):
    vmem = pl.BlockSpec(memory_space=pltpu.VMEM)
    hbm = pl.BlockSpec(memory_space=pl.ANY)
    dma = pltpu.SemaphoreType.DMA
    return pl.pallas_call(
        kernel,
        out_shape=jax.ShapeDtypeStruct((128, 2048), BF16),
        in_specs=[vmem, vmem] + [hbm] * 5 + [vmem, vmem] + [hbm] * 3 + [vmem, vmem] + [hbm] * 2,
        out_specs=vmem,
        scratch_shapes=[
            pltpu.VMEM((4, 128, 2048), BF16),
            pltpu.VMEM((2048, 1280), BF16),
            pltpu.VMEM((5, 512, 256), BF16),
            pltpu.VMEM((32, 2, 256, 256), BF16),
            pltpu.VMEM((32, 2, 288, 256), BF16),
            pltpu.VMEM((4, 2, 256, 2048), BF16),
            pltpu.VMEM((32, 8, 128), F32),
            pltpu.VMEM((256, 256), BF16),
            pltpu.VMEM((2, 4, 256, 256), BF16),
            pltpu.VMEM((2, 4, 128, 256), F32),
            pltpu.VMEM((2, 4, 1, 256), F32),
            pltpu.VMEM((2, 4, 1, 256), F32),
            pltpu.VMEM((2, 256, 256), BF16),
            pltpu.VMEM((2, 2, 256, 128), F32),
            pltpu.VMEM((2, 256, 256), BF16),
            pltpu.VMEM((512, 256), BF16),
            pltpu.VMEM((2, 4, 128, 256), BF16),
            dma((10,)),
            dma((6,)),
            dma((4, 2)),
            dma((7,)),
            dma((4, 3)),
            dma((16,)),
            dma((32,)),
            dma((16,)),
            dma((4, 10)),
            dma((32, 2, 2)),
            dma((32,)),
            dma((2,)),
            dma((8,)),
            dma((2, 4)),
        ],
        compiler_params=pltpu.CompilerParams(
            collective_id=0, has_side_effects=True, vmem_limit_bytes=60 * 1024 * 1024
        ),
        cost_estimate=pl.CostEstimate(
            flops=20_000_000_000, bytes_accessed=10_000_000, transcendentals=17_000_000
        ),
        name="layer",
    )(
        tokens, norm_gain.reshape(1, -1), w_query_one, w_query_two, w_key_one, w_key_two, w_value,
        jnp.broadcast_to(mix_lambda[:, None], (2, 256)), head_gain.reshape(1, -1),
        w_ret_query, w_ret_key, w_ret_value, retain_log, init_state, w_out_diff, w_out_ret,
    )


def solution(mesh):
    both = ("sp", "tp")
    return jax.shard_map(
        on_device,
        mesh=mesh,
        in_specs=(
            P(both, None), P(), P(None, "tp"), P(None, "tp"), P(None, "tp"), P(None, "tp"),
            P(None, "tp"), P("tp"), P(), P(None, "tp"), P(None, "tp"), P(None, "tp"),
            P("tp", "sp"), P("tp", None, None), P("tp", None), P("tp", None),
        ),
        out_specs=P(both, None),
        check_vma=False,
    )
```

time: 359 us -> 113 us (0.31)
  the two profiles are of different devices: /device:TPU:121 before, /device:TPU:71 now
where the time goes in v1:
time: 113 us; the launch traced here: 112 us
  Pallas kernels  109 us (96%)
  local copies, waits for them, and re-layouts  3.18 us (3%)
    pallas_call x1, Pallas kernels, on_device(): pl.pallas_call(kernel, out_shape=jax.ShapeDtypeStruct((128, 2048), BF16),...  109 us
    unnamed x3, local copies, waits for them, and re-layouts  2.54 us

profile of v1, /device:TPU:71, one launch (start us, length us, event | category | flops | bytes accessed | tf_op | source)
XLA Modules:
  0.0 112.3 jit_solution(17916454443181889936)
XLA Ops:
  0.0 0.0 copy-start
  0.0 0.7 copy-done
  0.7 0.6 broadcast_in_dim.2.mix
  1.3 109.2 %layer.1 = bf16[128,2048]{1,0:T(8,128)(2,1)} custom-call(bf16[128,2048]{1,0:T(8,128)(2,1)} %tokens.1, f32[1,2048]{1,0:T(1,128)} %bitcast.2, bf16[2048,128]{1,0:T(8,128)(2,1)} %wq1.1, bf16[2048,128]{1,0:T(8,128)(2,1)} %wq2.1, bf16[2048,128]{1,0:T(8,128)(2,1)} %wk1.1, bf16[2048,128]{1,0:T(8,128)(2,1)} %wk2.1, bf16[2048,256]{1,0:T(8,128)(2,1)} %wv.1, ...), custom_call_target="tpu_custom_call" | custom-call | flops 20000000000 | bytes 10000000 | tf_op jit(solution)/shard_map/layer/pallas_call | solution.py:620
  110.5 1.9 %copy.18 = bf16[128,2048]{1,0:T(8,128)(2,1)} copy(bf16[128,2048]{1,0:T(8,128)(2,1)} %layer.1) | data formatting | bytes 1048576
Async XLA Ops:
  0.0 0.7 copy-start
